TPU v7x, 32 devices: a whole 2x2x4 slice. The times are simulated.
32 devices in a mesh: sp: 8 (over z, x), tp: 4 (over y, core).
Axes of the slice: x: 2, y: 2, z: 4, core: 2. Of those that a mesh axis runs over, the one named last changes fastest.
Arguments:
- tokens: bfloat16 [2048, 3072], P('sp', 'tp'), may hold values from -6 to 6
- norm_gain: float32 [3072], replicated, may hold values from 0.1 to 1.9
- state_in_weight: bfloat16 [3072, 1024], P('sp', 'tp'), may hold values from -0.109375 to 0.109375
- pool_in_weight: bfloat16 [3072, 1024], P('sp', 'tp'), may hold values from -0.109375 to 0.109375
- rate_real: float32 [64, 64], replicated, may hold values from -1.5 to -0.5
- rate_imag: float32 [64, 64], replicated, may hold values from 0 to 200
- log_step: float32 [64], replicated, may hold values from -2 to 0.7
- input_real: float32 [64, 64, 16], replicated, may hold values from -1 to 1
- input_imag: float32 [64, 64, 16], replicated, may hold values from -1 to 1
- output_real: float32 [64, 16, 64], replicated, may hold values from -64 to 64
- output_imag: float32 [64, 16, 64], replicated, may hold values from -64 to 64
- skip_gain: float32 [1024], replicated, may hold values from -3 to 3
- pool_weight: bfloat16 [16, 64, 64], replicated, may hold values from -0.75 to 0.75
- pool_gain: float32 [1024], replicated, may hold values from 0.1 to 1.9
- state_out_weight: bfloat16 [1024, 3072], P('sp', 'tp'), may hold values from -0.125 to 0.125
- pool_out_weight: bfloat16 [1024, 3072], P('sp', 'tp'), may hold values from -0.125 to 0.125
Outputs:
- mixer_output: bfloat16 [2048, 3072], P('sp', 'tp')
All inputs are finite; a program needn't handle non-finite values.
Results may differ from a plain program's by a relative error of at most 0.0065.
Values may be sent and summed in bfloat16 or wider, within the bound.
A program may use at most 64 MiB of HBM per device.

v0:
```python
import jax
import jax.numpy as jnp
from jax import lax
from jax.sharding import PartitionSpec as P

SSM_GROUP = 16
POOL_GROUP = 64


epsilon = 1e-06
highest = lax.Precision.HIGHEST
window_reach = 16


def prefix(part, axis, combine, identity):
    place = lax.axis_index(axis)
    gathered = jax.tree.map(lambda a: lax.all_gather(a, axis), part)
    state = jax.tree.map(lambda a, e: jnp.zeros_like(a) + jnp.asarray(e, a.dtype), part, identity)

    def one(turn, state):
        return combine(
            state, jax.tree.map(lambda a: lax.dynamic_index_in_dim(a, turn, 0, False), gathered)
        )

    return lax.fori_loop(0, place, one, state)


def passed_along(value, axis, steps):
    count = lax.axis_size(axis)
    first, last = (max(0, -steps), min(count, count - steps))
    return lax.ppermute(value, axis, [(source, source + steps) for source in range(first, last)])


def discretize(rate_real, rate_imag, log_step, length):
    step_size = jnp.exp(log_step)[:, None] / length
    exponent = rate_real * step_size
    angle = rate_imag * step_size
    magnitude = jnp.exp(exponent)
    decay_real = magnitude * jnp.cos(angle)
    decay_imag = magnitude * jnp.sin(angle)
    less_one = jnp.expm1(exponent) * jnp.cos(angle) - 2.0 * jnp.square(jnp.sin(0.5 * angle))
    denominator = rate_real * rate_real + rate_imag * rate_imag
    factor_real = (less_one * rate_real + decay_imag * rate_imag) / denominator
    factor_imag = (decay_imag * rate_real - less_one * rate_imag) / denominator
    return (exponent, angle, decay_real, decay_imag, factor_real, factor_imag)


def complex_product(left_pair, right_pair):
    return jnp.stack(
        [
            left_pair[0] * right_pair[0] - left_pair[1] * right_pair[1],
            left_pair[0] * right_pair[1] + left_pair[1] * right_pair[0],
        ]
    )


def scan_combine(first_part, second_part):
    first_decay_real, first_decay_imag, first_real, first_imag = first_part
    second_decay_real, second_decay_imag, second_real, second_imag = second_part
    return (
        first_decay_real * second_decay_real - first_decay_imag * second_decay_imag,
        first_decay_real * second_decay_imag + first_decay_imag * second_decay_real,
        second_decay_real * first_real - second_decay_imag * first_imag + second_real,
        second_decay_real * first_imag + second_decay_imag * first_real + second_imag,
    )


def chain_combine(earlier, later):
    return (complex_product(later[0], earlier[0]), complex_product(later[0], earlier[1]) + later[1])


def local_slice(array, first_index, count_here):
    return lax.dynamic_slice_in_dim(array, first_index, count_here, 0)


def body(
    tokens,
    norm_gain,
    state_in_weight,
    pool_in_weight,
    rate_real,
    rate_imag,
    log_step,
    input_real,
    input_imag,
    output_real,
    output_imag,
    skip_gain,
    pool_weight,
    pool_gain,
    state_out_weight,
    pool_out_weight,
):
    state_in_full, pool_in_full, state_out_full, pool_out_full = (
        lax.all_gather(state_in_weight, "sp", axis=0, tiled=True),
        lax.all_gather(pool_in_weight, "sp", axis=0, tiled=True),
        lax.all_gather(state_out_weight, "sp", axis=0, tiled=True),
        lax.all_gather(pool_out_weight, "sp", axis=0, tiled=True),
    )
    row_count = tokens.shape[0]
    model_width = norm_gain.shape[0]
    state_width = state_in_full.shape[1]
    pool_width = pool_in_full.shape[1]
    features = lax.all_gather(tokens, "tp", axis=1, tiled=True).astype(jnp.float32)
    scaled = (features * norm_gain).astype(jnp.bfloat16)
    state_rows = state_in_full
    pool_rows = pool_in_full
    state_sum = jnp.dot(scaled, state_rows, preferred_element_type=jnp.float32)
    pool_sum = jnp.dot(scaled, pool_rows, preferred_element_type=jnp.float32)
    squares = jnp.sum(features * features, axis=1)
    state_sum, pool_sum, squares = (state_sum, pool_sum, squares)
    inverse = lax.rsqrt(squares / model_width + epsilon)[:, None]
    state_in = (state_sum * inverse).astype(jnp.bfloat16)
    pool_in = (pool_sum * inverse).astype(jnp.bfloat16)
    head_index = lax.axis_index("tp")
    block_index = lax.axis_index("sp")
    groups_here = state_width // SSM_GROUP
    first_group = head_index * groups_here
    length = row_count * lax.axis_size("sp")
    exponent, angle, decay_real, decay_imag, factor_real, factor_imag = discretize(
        local_slice(rate_real, first_group, groups_here),
        local_slice(rate_imag, first_group, groups_here),
        local_slice(log_step, first_group, groups_here),
        length,
    )
    state_columns = groups_here * decay_real.shape[1]
    exponent = exponent.reshape(state_columns)
    angle = angle.reshape(state_columns)
    decay_real = decay_real.reshape(state_columns)
    decay_imag = decay_imag.reshape(state_columns)
    group_identity = jnp.eye(groups_here, dtype=jnp.float32)
    local_in_real = local_slice(input_real, first_group, groups_here)
    local_in_imag = local_slice(input_imag, first_group, groups_here)
    drive_real = factor_real[..., None] * local_in_real - factor_imag[..., None] * local_in_imag
    drive_imag = factor_real[..., None] * local_in_imag + factor_imag[..., None] * local_in_real
    drive_matrix_real = jnp.einsum("gnc,gh->gchn", drive_real, group_identity).reshape(
        state_width, state_columns
    )
    drive_matrix_imag = jnp.einsum("gnc,gh->gchn", drive_imag, group_identity).reshape(
        state_width, state_columns
    )
    signal = state_in.astype(jnp.float32)
    push_real = jnp.dot(signal, drive_matrix_real, precision=highest)
    push_imag = jnp.dot(signal, drive_matrix_imag, precision=highest)
    decay_wide_real = jnp.broadcast_to(decay_real, push_real.shape)
    decay_wide_imag = jnp.broadcast_to(decay_imag, push_real.shape)
    _, _, local_real, local_imag = lax.associative_scan(
        scan_combine, (decay_wide_real, decay_wide_imag, push_real, push_imag), axis=0
    )
    end_state = jnp.stack([local_real[row_count - 1], local_imag[row_count - 1]])
    block_magnitude = jnp.exp(row_count * exponent)
    block_decay = jnp.stack(
        [block_magnitude * jnp.cos(row_count * angle), block_magnitude * jnp.sin(row_count * angle)]
    )
    last_rows = pool_in[row_count - window_reach :]
    identity = (
        jnp.stack([jnp.ones_like(exponent), jnp.zeros_like(exponent)]),
        jnp.zeros_like(end_state),
    )
    _, incoming = prefix((block_decay, end_state), "sp", chain_combine, identity)
    halo_block = passed_along(last_rows, "sp", 1)
    positions = (jnp.arange(row_count, dtype=jnp.float32) + 1.0)[:, None]
    power_magnitude = jnp.exp(positions * exponent[None, :])
    power_angle = positions * angle[None, :]
    power_cos = power_magnitude * jnp.cos(power_angle)
    power_sin = power_magnitude * jnp.sin(power_angle)
    states_real = local_real + power_cos * incoming[0] - power_sin * incoming[1]
    states_imag = local_imag + power_cos * incoming[1] + power_sin * incoming[0]
    local_out_real = local_slice(output_real, first_group, groups_here)
    local_out_imag = local_slice(output_imag, first_group, groups_here)
    read_matrix_real = jnp.einsum("gcn,gh->hngc", local_out_real, group_identity).reshape(
        state_columns, state_width
    )
    read_matrix_imag = jnp.einsum("gcn,gh->hngc", local_out_imag, group_identity).reshape(
        state_columns, state_width
    )
    readout_sum = jnp.dot(states_real, read_matrix_real, precision=highest)
    readout_sum = readout_sum - jnp.dot(states_imag, read_matrix_imag, precision=highest)
    readout_sum = (
        readout_sum + local_slice(skip_gain, head_index * state_width, state_width) * signal
    )
    state_out = jax.nn.gelu(readout_sum).astype(jnp.bfloat16)
    pool_groups_here = pool_width // POOL_GROUP
    first_pool = head_index * pool_groups_here
    extended = jnp.concatenate([halo_block, pool_in], axis=0)
    column_group = first_pool + jnp.arange(pool_width, dtype=jnp.int32) // POOL_GROUP
    column_window = jnp.left_shift(jnp.ones_like(column_group), column_group % 4 + 1)
    targets = jnp.arange(row_count, dtype=jnp.int32)[:, None] + window_reach
    sources = jnp.arange(row_count + window_reach, dtype=jnp.int32)[None, :]
    window_sums = jnp.zeros((row_count, pool_width), jnp.float32)
    for power_index in range(1, 5):
        span_width = 2**power_index
        band_mask = ((sources <= targets) & (sources > targets - span_width)).astype(jnp.bfloat16)
        partial_sums = jnp.dot(band_mask, extended, preferred_element_type=jnp.float32)
        window_sums = jnp.where(column_window[None, :] == span_width, partial_sums, window_sums)
    global_rows = block_index * row_count + jnp.arange(row_count, dtype=jnp.int32)
    divisor = jnp.minimum(global_rows[:, None] + 1, column_window[None, :]).astype(jnp.float32)
    pooled = window_sums / divisor - pool_in.astype(jnp.float32)
    pool_identity = jnp.eye(pool_groups_here, dtype=jnp.float32)
    mixer_matrix = jnp.einsum(
        "gcd,gh->gchd",
        local_slice(pool_weight, first_pool, pool_groups_here).astype(jnp.float32),
        pool_identity,
    ).reshape(pool_width, pool_width)
    projected = jnp.dot(pooled, mixer_matrix, precision=highest)
    pool_out = (projected * local_slice(pool_gain, head_index * pool_width, pool_width)).astype(
        jnp.bfloat16
    )
    state_rows = state_out_full
    pool_rows = pool_out_full
    running_sum = jnp.dot(
        lax.all_gather(state_out, "tp", axis=1, tiled=True),
        state_rows,
        preferred_element_type=jnp.float32,
    )
    combined = running_sum + jnp.dot(
        lax.all_gather(pool_out, "tp", axis=1, tiled=True),
        pool_rows,
        preferred_element_type=jnp.float32,
    )
    return combined.astype(jnp.bfloat16)


def solution(mesh):
    return jax.shard_map(
        body,
        mesh=mesh,
        in_specs=(
            P("sp", "tp"),
            P(),
            P("sp", "tp"),
            P("sp", "tp"),
            P(),
            P(),
            P(),
            P(),
            P(),
            P(),
            P(),
            P(),
            P(),
            P(),
            P("sp", "tp"),
            P("sp", "tp"),
        ),
        out_specs=P("sp", "tp"),
        check_vma=False,
    )
```

profile of v0, /device:TPU:25, one launch (start us, length us, event | category | flops | bytes accessed | tf_op | source)
XLA Modules:
  0.0 252.3 jit_solution(12776405410376965267)
XLA Ops:
  18.1 1.9 multiply_bitcast_fusion
  20.0 2.8 %reshape.307 = f32[1024,256]{0,1:T(8,128)} reshape(f32[16,64,16,16]{1,0,3,2:T(8,128)} %get-tuple-element.121) | data formatting | bytes 2097152 | tf_op jit(solution)/shard_map/reshape | solution.py:171
  23.8 2.6 %multiply_bitcast_fusion.2 = (f32[16,16,16,64]{3,2,1,0:T(8,128)}, f32[16,16,16,64]{3,2,1,0:T(8,128)}) fusion(f32[16,64,16]{1,2,0:T(8,128)S(1)} %get-tuple-element.81, f32[16,16]{1,0:T(8,128)S(1)} %fusion.78, f32[16,64,16]{1,2,0:T(8,128)S(1)} %get-tuple-element.82), kind=kLoop, calls=%fused_computation.11 | loop fusion | flops 524288 | bytes 2229248 | tf_op jit(solution)/shard_map/gnc,gh->gchn/transpose | solution.py:139
  26.3 2.0 reshape.306
  28.5 2.8 %reshape.303 = f32[256,1024]{1,0:T(8,128)} reshape(f32[16,16,16,64]{3,2,1,0:T(8,128)} %get-tuple-element.127) | data formatting | bytes 2097152 | tf_op jit(solution)/shard_map/reshape | solution.py:136
  32.8 23.6 %all-gather.2 = f32[8,2,1024]{2,1,0:T(2,128)} all-gather(f32[1,2,1024]{2,1,0:T(2,128)S(1)} %maximum_bitcast_fusion), channel_id=2, replica_groups=mesh['sp'=8,'tp'=4] {'sp'}, dimensions={0}, use_global_device_ids=true | all-gather | bytes 73728 | tf_op jit(solution)/shard_map/all_gather | solution.py:17
  65.0 1.9 fusion.1
  67.0 7.2 %all-gather.12.cloned.1.call-done = bf16[3072,256]{1,0:T(8,128)(2,1)} async-done(((bf16[384,256]{1,0:T(8,128)(2,1)}), bf16[3072,256]{1,0:T(8,128)(2,1)}) %all-gather.12.cloned.1.call-update) | async-done | bytes 1572880 | tf_op jit(solution)/shard_map/all_gather | solution.py:95
  74.2 2.0 fusion.20
  82.1 1.6 slice.380
  85.1 1.8 add_add_fusion.1
  90.0 2.0 add_add_fusion.3
  94.1 1.6 slice.395
  95.7 1.6 slice.399
  97.3 1.8 add_add_fusion.5
  103.5 1.6 add_add_fusion.7
  137.8 1.6 slice.456
  146.0 1.6 slice.474
  156.6 2.7 %pad.126 = f32[256,1024]{1,0:T(8,128)} pad(f32[128,1024]{1,0:T(8,128)S(1)} %pad_maximum_fusion, f32[]{:T(128)} %constant.91.clone.1), padding=0_1_1x0_0_0 | pad | bytes 1572868 | tf_op jit(solution)/shard_map/pad | solution.py:147
  159.4 2.7 %pad.127 = f32[256,1024]{1,0:T(8,128)} pad(f32[128,1024]{1,0:T(8,128)S(1)} %add.689, f32[]{:T(128)} %constant.91.clone.1), padding=1_0_1x0_0_0 | pad | bytes 1572868 | tf_op jit(solution)/shard_map/pad | solution.py:147
  162.1 2.7 %pad.129 = f32[256,1024]{1,0:T(8,128)} pad(f32[128,1024]{1,0:T(8,128)S(1)} %add.692, f32[]{:T(128)} %constant.91.clone.1), padding=1_0_1x0_0_0 | pad | bytes 1572868 | tf_op jit(solution)/shard_map/pad | solution.py:147
  164.9 2.7 %pad.128 = f32[256,1024]{1,0:T(8,128)} pad(f32[128,1024]{1,0:T(8,128)S(1)} %pad_maximum_fusion.1, f32[]{:T(128)} %constant.91.clone.1), padding=0_1_1x0_0_0 | pad | bytes 1572868 | tf_op jit(solution)/shard_map/pad | solution.py:147
  169.2 22.5 %all-gather.3 = f32[8,2,1024]{2,1,0:T(2,128)S(1)} all-gather(f32[1,2,1024]{2,1,0:T(2,128)S(1)} %maximum_bitcast_fusion.1), channel_id=3, replica_groups=mesh['sp'=8,'tp'=4] {'sp'}, dimensions={0}, use_global_device_ids=true | all-gather | bytes 73728 | tf_op jit(solution)/shard_map/all_gather | solution.py:17
  191.6 5.0 %while.12 = (s32[]{:T(128)}, f32[2,1024]{1,0:T(2,128)S(1)}, s32[]{:T(128)}, f32[8,2,1024]{2,1,0:T(2,128)}, f32[8,2,1024]{2,1,0:T(2,128)S(1)}, /*index=5*/s32[]{:T(128)}, s32[]{:T(128)}, s32[]{:T(128)}, s32[]{}) while((s32[]{:T(128)}, f32[2,1024]{1,0:T(2,128)S(1)}, s32[]{:T(128)}, f32[8,2,1024]{2,1,0:T(2,128)}, f32[8,2,1024]{2,1,0:T(2,128)S(1)}, ...), condition=%wide.region_2.3_spmd, body=%wide.region_1.2_spmd.sunk | while | flops 10246 | bytes 49311 | solution.py:25
  196.8 2.1 fusion.17
  199.0 5.8 %collective-permute-start = (bf16[16,256]{1,0:T(8,128)(2,1)S(1)}, bf16[16,256]{1,0:T(8,128)(2,1)S(1)}, u32[]{:S(2)}, u32[]{:S(2)}) collective-permute-start(bf16[16,256]{1,0:T(8,128)(2,1)S(1)} %slice.534), channel_id=1, source_target_pairs={{0,4},{4,8},{8,12},{12,16},{16,20},{20,24},{24,28},{1,5},{5,9},{9,... | collective-permute-start | bytes 24584 | tf_op jit(solution)/shard_map/ppermute | solution.py:31
  204.9 5.1 %fusion.29 = f32[256,256]{1,0:T(8,128)S(1)} fusion(f32[1024,256]{0,1:T(8,128)S(1)} %copy-done.12, f32[256,1024]{1,0:T(8,128)S(1)} %copy-done.9, f32[256,1024]{1,0:T(8,128)S(1)} %copy-done.11, f32[1024]{0:T(1024)S(1)} %bitcast.64, f32[1024]{0:T(1024)S(1)} %bitcast.62, f32[1024]{0:T(1024)S(1)} %copy-done.52, f32[1024]{0:T(1024)S(1)} %copy-done.53, ...), kind=kOutput, calls=%fused_computation.39 | convolution fusion | flops 807665664 | bytes 3425280 | tf_op jit(solution)/shard_map/dot_general | solution.py:177
  210.0 5.1 %fusion.67 = bf16[256,256]{1,0:T(8,128)(2,1)S(1)} fusion(f32[256,256]{1,0:T(8,128)S(1)} %fusion.29, f32[1024,256]{0,1:T(8,128)S(1)} %copy-done.13, f32[256,1024]{1,0:T(8,128)S(1)} %copy-done.10, f32[256,1024]{1,0:T(8,128)S(1)} %copy-done.8, f32[1024]{0:T(1024)S(1)} %bitcast.65, f32[1024]{0:T(1024)S(1)} %bitcast.63, f32[1024]{0:T(1024)S(1)} %copy-done.52, ...), kind=kOutput, calls=%fused_computation.83 | convolution fusion | flops 808517632 | bytes 3688448 | tf_op jit(solution)/shard_map/dot_general | solution.py:178
  215.2 16.8 %all_gather.39 = bf16[256,1024]{1,0:T(8,128)(2,1)S(1)} all-gather(bf16[256,256]{1,0:T(8,128)(2,1)S(1)} %fusion.67), channel_id=1, replica_groups=mesh['sp'=8,'tp'=4] {'tp'}, dimensions={1}, use_global_device_ids=true | all-gather | bytes 655360 | tf_op jit(solution)/shard_map/all_gather | solution.py:212
  232.1 2.0 fusion.93
  235.8 7.3 %all_gather.42 = bf16[256,1024]{1,0:T(8,128)(2,1)S(1)} all-gather(bf16[256,256]{1,0:T(8,128)(2,1)S(1)} %fusion.16), channel_id=1, replica_groups=mesh['sp'=8,'tp'=4] {'tp'}, dimensions={1}, use_global_device_ids=true | all-gather | bytes 655360 | tf_op jit(solution)/shard_map/all_gather | solution.py:217
  243.1 2.7 %fusion.6 = bf16[256,768]{1,0:T(8,128)(2,1)} fusion(f32[256,768]{1,0:T(8,128)S(1)} %fusion.93, bf16[256,1024]{1,0:T(8,128)(2,1)S(1)} %all_gather.42, bf16[1024,768]{1,0:T(8,128)(2,1)} %all-gather.18.cloned.1.call-done), kind=kOutput, calls=%fused_computation.18 | convolution fusion | flops 403046400 | bytes 3276800 | tf_op jit(solution)/shard_map/dot_general | solution.py:216
  (323 shorter events, 95.6 us)
Async XLA Ops:
  6.5 58.5 %all-gather.10.cloned.1.call-start = ((), (), s32[]{:S(2)}) async-start(), calls=%async_computation | async-start | bytes 1966080 | tf_op jit(solution)/shard_map/all_gather | solution.py:104
  7.3 66.9 %all-gather.12.cloned.1.call-start = ((), (), s32[]{:S(2)}) async-start(), calls=%async_computation.1 | async-start | bytes 1769472 | tf_op jit(solution)/shard_map/all_gather | solution.py:95
  8.0 188.7 %all-gather.16.cloned.1.call-start = ((), (), s32[]{:S(2)}) async-start(), calls=%async_computation.3 | async-start | bytes 1769472 | tf_op jit(solution)/shard_map/all_gather | solution.py:96
  8.7 223.3 %all-gather.14.cloned.1.call-start = ((), (), s32[]{:S(2)}) async-start(), calls=%async_computation.2 | async-start | bytes 1769472 | tf_op jit(solution)/shard_map/all_gather | solution.py:97
  9.3 233.7 %all-gather.18.cloned.1.call-start = ((), (), s32[]{:S(2)}) async-start(), calls=%async_computation.4 | async-start | bytes 1769472 | tf_op jit(solution)/shard_map/all_gather | solution.py:98
  28.4 56.7 %copy-start.25 = (f32[1024]{0:T(1024)}, f32[1024]{0:T(1024)S(1)}, u32[]{:S(2)}) copy-start(f32[1024]{0:T(1024)S(1)} %reshape.305) | copy-start | bytes 12292
  28.5 56.7 %copy-start.27 = (f32[1024]{0:T(1024)}, f32[1024]{0:T(1024)S(1)}, u32[]{:S(2)}) copy-start(f32[1024]{0:T(1024)S(1)} %reshape.304) | copy-start | bytes 12292
  59.3 14.8 %copy-start.61 = (f32[3072]{0:T(1024)S(1)}, f32[3072]{0:T(1024)}, u32[]{:S(2)}) copy-start(f32[3072]{0:T(1024)} %param.19) | copy-start | bytes 36868
  63.9 26.2 %copy-start.29 = (f32[1024]{0:T(1024)}, f32[1024]{0:T(1024)S(1)}, u32[]{:S(2)}) copy-start(f32[1024]{0:T(1024)S(1)} %get-tuple-element.72) | copy-start | bytes 12292
  63.9 26.2 %copy-start.31 = (f32[1024]{0:T(1024)}, f32[1024]{0:T(1024)S(1)}, u32[]{:S(2)}) copy-start(f32[1024]{0:T(1024)S(1)} %get-tuple-element.73) | copy-start | bytes 12292
  63.9 33.5 %copy-start.33 = (f32[1024]{0:T(1024)}, f32[1024]{0:T(1024)S(1)}, u32[]{:S(2)}) copy-start(f32[1024]{0:T(1024)S(1)} %get-tuple-element.70) | copy-start | bytes 12292
  63.9 33.5 %copy-start.35 = (f32[1024]{0:T(1024)}, f32[1024]{0:T(1024)S(1)}, u32[]{:S(2)}) copy-start(f32[1024]{0:T(1024)S(1)} %get-tuple-element.71) | copy-start | bytes 12292
  63.9 39.6 %copy-start.37 = (f32[1024]{0:T(1024)}, f32[1024]{0:T(1024)S(1)}, u32[]{:S(2)}) copy-start(f32[1024]{0:T(1024)S(1)} %get-tuple-element.68) | copy-start | bytes 12292
  63.9 39.6 %copy-start.39 = (f32[1024]{0:T(1024)}, f32[1024]{0:T(1024)S(1)}, u32[]{:S(2)}) copy-start(f32[1024]{0:T(1024)S(1)} %get-tuple-element.69) | copy-start | bytes 12292
  65.0 9.1 %copy-start.6 = (bf16[256,3072]{1,0:T(8,128)(2,1)S(1)}, bf16[256,3072]{1,0:T(8,128)(2,1)}, u32[]{:S(2)}) copy-start(bf16[256,3072]{1,0:T(8,128)(2,1)} %all-gather.10.cloned.1.call-done) | copy-start | bytes 4718596
  67.0 9.2 %copy-start.59 = (f32[256]{0:T(256)}, f32[256]{0:T(256)S(1)}, u32[]{:S(2)}) copy-start(f32[256]{0:T(256)S(1)} %add_rsqrt_fusion) | copy-start | bytes 3076
  76.9 70.7 %copy-start = (f32[256,1024]{1,0:T(8,128)}, f32[256,1024]{1,0:T(8,128)S(1)}, u32[]{:S(2)}) copy-start(f32[256,1024]{1,0:T(8,128)S(1)} %fusion.92) | copy-start | bytes 3145732
  82.0 65.5 %copy-start.1 = (f32[256,1024]{1,0:T(8,128)}, f32[256,1024]{1,0:T(8,128)S(1)}, u32[]{:S(2)}) copy-start(f32[256,1024]{1,0:T(8,128)S(1)} %fusion.91) | copy-start | bytes 3145732
  145.9 5.8 %copy-start.19 = (f32[15,1024]{1,0:T(8,128)S(1)}, f32[15,1024]{1,0:T(8,128)}, u32[]{:S(2)}) copy-start(f32[15,1024]{1,0:T(8,128)} %slice.460) | copy-start | bytes 184324
  145.9 5.8 %copy-start.20 = (f32[15,1024]{1,0:T(8,128)S(1)}, f32[15,1024]{1,0:T(8,128)}, u32[]{:S(2)}) copy-start(f32[15,1024]{1,0:T(8,128)} %slice.456) | copy-start | bytes 184324
  145.9 5.8 %copy-start.38 = (f32[1024]{0:T(1024)S(1)}, f32[1024]{0:T(1024)}, u32[]{:S(2)}) copy-start(f32[1024]{0:T(1024)} %copy-done.37) | copy-start | bytes 12292
  146.0 5.8 %copy-start.40 = (f32[1024]{0:T(1024)S(1)}, f32[1024]{0:T(1024)}, u32[]{:S(2)}) copy-start(f32[1024]{0:T(1024)} %copy-done.39) | copy-start | bytes 12292
  164.8 31.9 %copy-start.7 = (bf16[256,3072]{1,0:T(8,128)(2,1)S(1)}, bf16[256,3072]{1,0:T(8,128)(2,1)}, u32[]{:S(2)}) copy-start(bf16[256,3072]{1,0:T(8,128)(2,1)} %all-gather.10.cloned.1.call-done) | copy-start | bytes 4718596
  164.8 32.0 %copy-start.60 = (f32[256]{0:T(256)S(1)}, f32[256]{0:T(256)}, u32[]{:S(2)}) copy-start(f32[256]{0:T(256)} %copy-done.59) | copy-start | bytes 3076
  164.8 32.0 %copy-start.62 = (f32[3072]{0:T(1024)S(1)}, f32[3072]{0:T(1024)}, u32[]{:S(2)}) copy-start(f32[3072]{0:T(1024)} %param.19) | copy-start | bytes 36868
  196.7 8.1 %copy-start.9 = (f32[256,1024]{1,0:T(8,128)S(1)}, f32[256,1024]{1,0:T(8,128)}, u32[]{:S(2)}) copy-start(f32[256,1024]{1,0:T(8,128)} %pad.126) | copy-start | bytes 3145732
  196.7 8.1 %copy-start.52 = (f32[1024]{0:T(1024)S(1)}, f32[1024]{0:T(1024)}, u32[]{:S(2)}) copy-start(f32[1024]{0:T(1024)} %mul.1012) | copy-start | bytes 12292
  196.7 8.1 %copy-start.53 = (f32[1024]{0:T(1024)S(1)}, f32[1024]{0:T(1024)}, u32[]{:S(2)}) copy-start(f32[1024]{0:T(1024)} %mul.1009) | copy-start | bytes 12292
  196.7 8.1 %copy-start.69 = (f32[256]{0:T(256)S(1)}, f32[256]{0:T(256)}, u32[]{:S(2)}) copy-start(f32[256]{0:T(256)} %iota_add_fusion.4) | copy-start | bytes 3076
  196.8 8.1 %copy-start.11 = (f32[256,1024]{1,0:T(8,128)S(1)}, f32[256,1024]{1,0:T(8,128)}, u32[]{:S(2)}) copy-start(f32[256,1024]{1,0:T(8,128)} %pad.127) | copy-start | bytes 3145732
  196.8 8.1 %copy-start.12 = (f32[1024,256]{0,1:T(8,128)S(1)}, f32[1024,256]{0,1:T(8,128)}, u32[]{:S(2)}) copy-start(f32[1024,256]{0,1:T(8,128)} %reshape.307) | copy-start | bytes 3145732
  199.0 35.1 %collective-permute-start = (bf16[16,256]{1,0:T(8,128)(2,1)S(1)}, bf16[16,256]{1,0:T(8,128)(2,1)S(1)}, u32[]{:S(2)}, u32[]{:S(2)}) collective-permute-start(bf16[16,256]{1,0:T(8,128)(2,1)S(1)} %slice.534), channel_id=1, source_target_pairs={{0,4},{4,8},{8,12},{12,16},{16,20},{20,24},{24,28},{1,5},{5,9},{9,... | collective-permute-start | bytes 24584 | tf_op jit(solution)/shard_map/ppermute | solution.py:31
  (46 other events, 128.3 us)
Sparse Core Ops, SparseCore 0:
  8.9 21.0 all-gather.9
  32.1 42.0 all-gather.11
  76.4 42.4 all-gather.15
  120.9 42.5 all-gather.13
  165.5 42.8 all-gather.17
where the time goes:
time: 255 us; the launch traced here: 252 us
  local copies, waits for them, and re-layouts  89.1 us (35%)
  blocking collectives  70.1 us (27%)
  other arithmetic  40.2 us (16%)
  matrix products  21.9 us (9%)
  between operations  14.5 us (6%)
  waiting for transfers between devices  10.4 us (4%)
  starting transfers between devices  5.98 us (2%)
    slice x54, local copies, waits for them, and re-layouts, body(): lax.associative_scan(scan_combine, (decay_wide_real, decay_wide_imag, pus...  56.2 us
    all_gather x2, blocking collectives, prefix(): gathered = jax.tree.map(lambda a: lax.all_gather(a, axis), part)  46 us
    all_gather x1, blocking collectives, body(): lax.all_gather(state_out, 'tp', axis=1, tiled=True)  16.8 us
    add x13, other arithmetic, scan_combine(): second_decay_real * first_imag + second_decay_imag * first_real  13.6 us
    pad x28, local copies, waits for them, and re-layouts, body(): lax.associative_scan(scan_combine, (decay_wide_real, decay_wide_imag, pus...  13 us
    all_gather x1, blocking collectives, body(): lax.all_gather(pool_out, 'tp', axis=1, tiled=True)  7.28 us
    all_gather x1, waiting for transfers between devices, body(): lax.all_gather(state_in_weight, 'sp', axis=0, tiled=True)  7.19 us
    ppermute x1, starting transfers between devices, passed_along(): lax.ppermute(value, axis, [(source, source + steps) for source in range(f...  5.83 us
  transfers between devices with their start and end apart: 6, of which 1 were waited for; matrix products, arithmetic and copies ran while one was open for 58% of the time, Pallas kernels for 0%

commit v1 on v0

v1 whole, which is shorter than its diff:
```python
import functools

import jax
import jax.numpy as jnp
from jax import lax
from jax.experimental import pallas as pl
from jax.experimental.pallas import tpu as pltpu
from jax.sharding import PartitionSpec as P

SSM_GROUP = 16
POOL_GROUP = 64
CHUNKS = 8
PIECES = 2

epsilon = 1e-06
window_reach = 16
f32, bf16 = jnp.float32, jnp.bfloat16
MESH = pl.DeviceIdType.MESH


def discretize(rate_real, rate_imag, log_step, length):
    step_size = jnp.exp(log_step)[:, None] / length
    exponent = rate_real * step_size
    angle = rate_imag * step_size
    magnitude = jnp.exp(exponent)
    decay_real = magnitude * jnp.cos(angle)
    decay_imag = magnitude * jnp.sin(angle)
    less_one = jnp.expm1(exponent) * jnp.cos(angle) - 2.0 * jnp.square(jnp.sin(0.5 * angle))
    denominator = rate_real * rate_real + rate_imag * rate_imag
    factor_real = (less_one * rate_real + decay_imag * rate_imag) / denominator
    factor_imag = (decay_imag * rate_real - less_one * rate_imag) / denominator
    return decay_real, decay_imag, factor_real, factor_imag


def iota(shape, axis):
    return lax.broadcasted_iota(jnp.int32, shape, axis)


def dot(a, b):
    return jnp.dot(a, b, preferred_element_type=f32)


def dot_nt(a, b):
    return lax.dot_general(a, b, (((1,), (1,)), ((), ())), preferred_element_type=f32)


def split(a):
    high = a.astype(bf16)
    return high, (a - high.astype(f32)).astype(bf16)


def cmul(ar, ai, br, bi):
    return ar * br - ai * bi, ar * bi + ai * br


def kernel(
    n_sp, n_tp, n_x, states,
    tok_ref, gain_ref, wsi_ref, wpi_ref, dec_ref, drive_ref, read_ref, skip_ref, pw_ref, pg_ref,
    wso_ref, wpo_ref,
    out_ref,
    tok_full, wsi, wpi, wso, wpo, scaled, dmat, rmat, pmat, push, ext, halo, ends, act,
    mine_s, mine_p, halo_out,
    own_sem, ring_send, ring_recv, tok_send, tok_recv, act_send, act_recv, halo_sem, end_send, end_recv,
):
    me, tp = lax.axis_index("sp"), lax.axis_index("tp")
    n_z = n_sp // n_x
    rows = tok_ref.shape[0]
    features = tok_ref.shape[1]
    width = wsi_ref.shape[1]
    pool_width = wpi_ref.shape[1]
    columns = dec_ref.shape[1]
    span = rows // CHUNKS

    def place(p):
        x, r = p // n_z, p % n_z
        return (r + (x % 2) * (n_z - 1 - 2 * r)) * n_x + x

    my_x, my_z = me % n_x, me // n_x
    at = my_x * n_z + my_z + (my_x % 2) * (n_z - 1 - 2 * my_z)

    barrier = pltpu.get_barrier_semaphore()
    for k in range(1, n_sp):
        pl.semaphore_signal(barrier, inc=1, device_id=((me + k) % n_sp, tp), device_id_type=MESH)
    for k in range(1, n_tp):
        pl.semaphore_signal(barrier, inc=1, device_id=(me, (tp + k) % n_tp), device_id_type=MESH)

    fulls = ((wsi_ref, wsi), (wpi_ref, wpi), (wso_ref, wso), (wpo_ref, wpo))
    owns = []
    for a, (own, full) in enumerate(fulls):
        count = own.shape[0]
        owns.append(
            pltpu.make_async_copy(
                own, full.at[pl.ds(pl.multiple_of(me * count, count), count)], own_sem.at[a]
            )
        )
    owns.append(pltpu.make_async_copy(tok_ref, tok_full.at[tp], own_sem.at[4]))
    for c in owns:
        c.start()
    pl.semaphore_wait(barrier, n_sp - 1 + n_tp - 1)

    def part(a, s, h):
        own, full = fulls[a]
        count = own.shape[0]
        size = count // PIECES
        way = 1 if a % 2 == 0 else -1
        owner = place((at - way * s + n_sp) % n_sp)
        there = full.at[pl.ds(pl.multiple_of(owner * count + h * size, size), size)]
        source = own.at[pl.ds(h * size, size)] if s == 0 else there
        return source, there, (place((at + way + n_sp) % n_sp), tp)

    def sender(a, s, h):
        source, there, target = part(a, s, h)
        return pltpu.make_async_remote_copy(
            source, there, ring_send.at[a, s, h], ring_recv.at[a, s, h],
            device_id=target, device_id_type=MESH,
        )

    def arrive(a, s, h):
        _, there, target = part(a, s + 1, h)
        pltpu.make_async_remote_copy(
            there, there, ring_send.at[a, s, h], ring_recv.at[a, s, h],
            device_id=target, device_id_type=MESH,
        ).wait_recv()

    last = n_sp - 2

    def ring(phase, s):
        for h in range(PIECES):
            for a in (2 * phase, 2 * phase + 1):
                arrive(a, s, h)
                if s < last:
                    sender(a, s + 1, h).start()
                    if s + 1 == last and phase == 0:
                        sender(a + 2, 0, h).start()

    def token_copy(k):
        return pltpu.make_async_remote_copy(
            tok_ref, tok_full.at[tp], tok_send.at[k - 1], tok_recv.at[k - 1],
            device_id=(me, (tp + k) % n_tp), device_id_type=MESH,
        )

    for h in range(PIECES):
        for a in (0, 1):
            sender(a, 0, h).start()
    for k in range(1, n_tp):
        token_copy(k).start()

    def build_drive(i):
        spread = (iota((width, SSM_GROUP), 0) % SSM_GROUP == iota((width, SSM_GROUP), 1)).astype(bf16)
        same = iota((width, columns), 0) // SSM_GROUP == iota((width, columns), 1) // states
        for j, piece in enumerate(split(drive_ref[i])):
            dmat[i, j] = jnp.where(same, dot_nt(spread, piece), 0.0).astype(bf16)

    def build_read(i):
        spread = (iota((columns, states), 0) % states == iota((columns, states), 1)).astype(bf16)
        same = iota((columns, width), 0) // states == iota((columns, width), 1) // SSM_GROUP
        for j, piece in enumerate(split(read_ref[i])):
            rmat[i, j] = jnp.where(same, dot_nt(spread, piece), 0.0).astype(bf16)

    def build_pool():
        spread = (
            iota((POOL_GROUP, pool_width), 0) == iota((POOL_GROUP, pool_width), 1) % POOL_GROUP
        ).astype(bf16)
        same = iota((pool_width, pool_width), 0) // POOL_GROUP == iota((pool_width, pool_width), 1) // POOL_GROUP
        pmat[...] = jnp.where(same, dot(pw_ref[...], spread), 0.0).astype(bf16)

    first = [
        lambda: build_drive(0), lambda: build_drive(1), lambda: build_read(0),
        lambda: build_read(1), build_pool,
    ]
    squares = []

    def take(t):
        block = tok_full[t].astype(f32)
        squares.append(jnp.sum(block * block, axis=1, keepdims=True))
        cut = slice(t * features, (t + 1) * features)
        scaled[:, cut] = (block * gain_ref[:, cut]).astype(bf16)

    def tokens_in():
        owns[4].wait()
        for k in range(1, n_tp):
            pltpu.make_async_remote_copy(
                tok_ref, tok_full.at[(tp - k + n_tp) % n_tp], tok_send.at[k - 1], tok_recv.at[k - 1],
                device_id=(me, (tp + k) % n_tp), device_id_type=MESH,
            ).wait_recv()

    for s in range(n_sp - 1):
        if s < len(first):
            first[s]()
        ring(0, s)
    for rest in first[n_sp - 1 :]:
        rest()
    tokens_in()
    for t in range(n_tp):
        take(t)
    owns[0].wait()
    owns[1].wait()
    inverse = lax.rsqrt(sum(squares) / (features * n_tp) + epsilon)
    pool_in = (dot(scaled[...], wpi[...]) * inverse).astype(bf16)
    ext[window_reach:] = pool_in
    halo_out[...] = pool_in[rows - window_reach :]
    state_in = (dot(scaled[...], wsi[...]) * inverse).astype(bf16)
    halo_copy = pltpu.make_async_remote_copy(
        halo_out, halo, halo_sem.at[0], halo_sem.at[1],
        device_id=((me + 1) % n_sp, tp), device_id_type=MESH,
    )
    halo_copy.start()
    done = [0]

    def step():
        if done[0] < n_sp - 1:
            ring(1, done[0])
            done[0] += 1

    step()
    shuffle = (
        iota((rows, rows), 1)
        == (iota((rows, rows), 0) % CHUNKS) * span + iota((rows, rows), 0) // CHUNKS
    ).astype(bf16)
    signal = dot(shuffle, state_in).astype(bf16)
    for i in range(2):
        push[i] = dot(signal, dmat[i, 0]) + dot(signal, dmat[i, 1])
    step()
    decay_real = jnp.broadcast_to(dec_ref[0:1, :], (CHUNKS, columns))
    decay_imag = jnp.broadcast_to(dec_ref[1:2, :], (CHUNKS, columns))

    def advance(p, carry):
        cut = pl.ds(pl.multiple_of(p * CHUNKS, CHUNKS), CHUNKS)
        real, imag = cmul(decay_real, decay_imag, *carry)
        real, imag = real + push[0, cut, :], imag + push[1, cut, :]
        push[0, cut, :] = real
        push[1, cut, :] = imag
        return real, imag

    zero = jnp.zeros((CHUNKS, columns), f32)
    end_real, end_imag = lax.fori_loop(0, span, advance, (zero, zero))

    def power(real, imag, count):
        out = None
        while count:
            if count % 2:
                out = (real, imag) if out is None else cmul(*out, real, imag)
            real, imag = cmul(real, imag, real, imag)
            count //= 2
        return out

    chunk_decay = power(dec_ref[0:1, :], dec_ref[1:2, :], span)
    block_decay = power(*chunk_decay, CHUNKS)
    row_zero = jnp.zeros((1, columns), f32)
    total = (row_zero, row_zero)
    for j in range(CHUNKS):
        moved = cmul(*chunk_decay, *total)
        total = (moved[0] + end_real[j : j + 1], moved[1] + end_imag[j : j + 1])
    which = iota((CHUNKS, columns), 0)
    ends[me] = jnp.where(which == 0, total[0], jnp.where(which == 1, total[1], 0.0))
    step()

    def end_copy(k):
        return pltpu.make_async_remote_copy(
            ends.at[me], ends.at[me], end_send.at[k - 1], end_recv.at[k - 1],
            device_id=((me + k) % n_sp, tp), device_id_type=MESH,
        )

    for k in range(1, n_sp):
        end_copy(k).start()

    halo_copy.wait_recv()
    ext[:window_reach] = jnp.where(me == 0, jnp.zeros_like(halo), halo[...])
    group = tp * (pool_width // POOL_GROUP) + iota((rows, pool_width), 1) // POOL_GROUP
    window = jnp.left_shift(jnp.ones_like(group), group % 4 + 1)
    targets = iota((rows, rows + window_reach), 0) + window_reach
    sources = iota((rows, rows + window_reach), 1)
    whole = ext[...]
    sums = jnp.zeros((rows, pool_width), f32)
    for power_index in range(1, 5):
        reach = 2**power_index
        band = ((sources <= targets) & (sources > targets - reach)).astype(bf16)
        sums = jnp.where(window == reach, dot(band, whole), sums)
    position = me * rows + iota((rows, pool_width), 0)
    divisor = jnp.minimum(position + 1, window).astype(f32)
    pooled = sums / divisor - ext[window_reach:].astype(f32)
    pooled_high, pooled_low = split(pooled)
    projected = dot(pooled_high, pmat[...]) + dot(pooled_low, pmat[...])
    mine_p[...] = (projected * pg_ref[...]).astype(bf16)
    step()

    def act_copy(which, k, source):
        mine = mine_s if which == 0 else mine_p
        return pltpu.make_async_remote_copy(
            mine, act.at[which, source], act_send.at[which, k - 1], act_recv.at[which, k - 1],
            device_id=(me, (tp + k) % n_tp), device_id_type=MESH,
        )

    for k in range(1, n_tp):
        act_copy(1, k, tp).start()
    act[1, tp] = mine_p[...]

    for k in range(1, n_sp):
        there = ends.at[(me - k + n_sp) % n_sp]
        pltpu.make_async_remote_copy(
            there, there, end_send.at[k - 1], end_recv.at[k - 1],
            device_id=((me + k) % n_sp, tp), device_id_type=MESH,
        ).wait_recv()
    total = (row_zero, row_zero)
    for s in range(n_sp - 1):
        moved = cmul(*block_decay, *total)
        use = s < me
        total = (
            jnp.where(use, moved[0] + ends[s, 0:1, :], total[0]),
            jnp.where(use, moved[1] + ends[s, 1:2, :], total[1]),
        )
    begin_real, begin_imag = zero, zero
    for j in range(CHUNKS):
        begin_real = jnp.where(which == j, total[0], begin_real)
        begin_imag = jnp.where(which == j, total[1], begin_imag)
        moved = cmul(*chunk_decay, *total)
        total = (moved[0] + end_real[j : j + 1], moved[1] + end_imag[j : j + 1])

    def add_carry(p, carry):
        cut = pl.ds(pl.multiple_of(p * CHUNKS, CHUNKS), CHUNKS)
        real, imag = cmul(decay_real, decay_imag, *carry)
        push[0, cut, :] = push[0, cut, :] + real
        push[1, cut, :] = push[1, cut, :] + imag
        return real, imag

    lax.fori_loop(0, span, add_carry, (begin_real, begin_imag))
    step()
    real_high, real_low = split(push[0])
    imag_high, imag_low = split(push[1])
    readout = dot(real_high, rmat[0, 0]) + dot(real_high, rmat[0, 1]) + dot(real_low, rmat[0, 0])
    readout -= dot(imag_high, rmat[1, 0]) + dot(imag_high, rmat[1, 1]) + dot(imag_low, rmat[1, 0])
    readout += skip_ref[...] * signal.astype(f32)
    shuffled = jax.nn.gelu(readout).astype(bf16)
    restore = (
        iota((rows, rows), 0)
        == (iota((rows, rows), 1) % CHUNKS) * span + iota((rows, rows), 1) // CHUNKS
    ).astype(bf16)
    mine_s[...] = dot(restore, shuffled).astype(bf16)
    step()
    for k in range(1, n_tp):
        act_copy(0, k, tp).start()
    act[0, tp] = mine_s[...]
    while done[0] < n_sp - 1:
        step()
    for which in (1, 0):
        for k in range(1, n_tp):
            act_copy(which, k, (tp - k + n_tp) % n_tp).wait_recv()
    owns[2].wait()
    owns[3].wait()
    result = None
    for t in range(n_tp):
        for which, full, size in ((1, wpo, pool_width), (0, wso, width)):
            term = dot(act[which, t], full[t * size : (t + 1) * size, :])
            result = term if result is None else result + term
    out_ref[...] = result.astype(bf16)

    for a in range(4):
        for s in range(n_sp - 1):
            for h in range(PIECES):
                sender(a, s, h).wait_send()
    for k in range(1, n_tp):
        token_copy(k).wait_send()
        act_copy(0, k, tp).wait_send()
        act_copy(1, k, tp).wait_send()
    halo_copy.wait_send()
    for k in range(1, n_sp):
        end_copy(k).wait_send()


def body(
    n_sp, n_tp, n_x,
    tokens, norm_gain, state_in_weight, pool_in_weight, rate_real, rate_imag, log_step,
    input_real, input_imag, output_real, output_imag, skip_gain, pool_weight, pool_gain,
    state_out_weight, pool_out_weight,
):
    rows, features = tokens.shape
    in_rows, width = state_in_weight.shape
    pool_width = pool_in_weight.shape[1]
    out_rows, out_columns = state_out_weight.shape
    groups = width // SSM_GROUP
    states = rate_real.shape[1]
    columns = groups * states
    pool_groups = pool_width // POOL_GROUP
    tp = lax.axis_index("tp")

    def mine(a, count):
        return lax.dynamic_slice_in_dim(a, tp * count, count, 0)

    decay_real, decay_imag, factor_real, factor_imag = discretize(
        mine(rate_real, groups), mine(rate_imag, groups), mine(log_step, groups), rows * n_sp
    )
    local_real, local_imag = mine(input_real, groups), mine(input_imag, groups)
    drive = jnp.stack(
        [
            factor_real[..., None] * local_real - factor_imag[..., None] * local_imag,
            factor_real[..., None] * local_imag + factor_imag[..., None] * local_real,
        ]
    ).reshape(2, columns, SSM_GROUP)
    read = jnp.stack([mine(output_real, groups), mine(output_imag, groups)]).reshape(2, width, states)
    decay = jnp.stack([decay_real, decay_imag]).reshape(2, columns)
    pool_matrix = mine(pool_weight, pool_groups).reshape(pool_width, POOL_GROUP)
    vmem = pl.BlockSpec(memory_space=pltpu.VMEM)
    dma = pltpu.SemaphoreType.DMA
    return pl.pallas_call(
        functools.partial(kernel, n_sp, n_tp, n_x, states),
        out_shape=jax.ShapeDtypeStruct((rows, out_columns), bf16),
        in_specs=[vmem] * 12,
        out_specs=vmem,
        scratch_shapes=[
            pltpu.VMEM((n_tp, rows, features), bf16),
            pltpu.VMEM((n_sp * in_rows, width), bf16),
            pltpu.VMEM((n_sp * in_rows, pool_width), bf16),
            pltpu.VMEM((n_sp * out_rows, out_columns), bf16),
            pltpu.VMEM((n_sp * out_rows, out_columns), bf16),
            pltpu.VMEM((rows, features * n_tp), bf16),
            pltpu.VMEM((2, 2, width, columns), bf16),
            pltpu.VMEM((2, 2, columns, width), bf16),
            pltpu.VMEM((pool_width, pool_width), bf16),
            pltpu.VMEM((2, rows, columns), f32),
            pltpu.VMEM((rows + window_reach, pool_width), bf16),
            pltpu.VMEM((window_reach, pool_width), bf16),
            pltpu.VMEM((n_sp, CHUNKS, columns), f32),
            pltpu.VMEM((2, n_tp, rows, width), bf16),
            pltpu.VMEM((rows, width), bf16),
            pltpu.VMEM((rows, pool_width), bf16),
            pltpu.VMEM((window_reach, pool_width), bf16),
            dma((5,)),
            dma((4, n_sp - 1, PIECES)),
            dma((4, n_sp - 1, PIECES)),
            dma((n_tp - 1,)),
            dma((n_tp - 1,)),
            dma((2, n_tp - 1)),
            dma((2, n_tp - 1)),
            dma((2,)),
            dma((n_sp - 1,)),
            dma((n_sp - 1,)),
        ],
        compiler_params=pltpu.CompilerParams(
            collective_id=0, has_side_effects=True, vmem_limit_bytes=60 * 2**20
        ),
    )(
        tokens, norm_gain[None], state_in_weight, pool_in_weight, decay, drive, read,
        mine(skip_gain, width)[None], pool_matrix, mine(pool_gain, pool_width)[None],
        state_out_weight, pool_out_weight,
    )


def solution(mesh):
    n_sp, n_tp = mesh.shape["sp"], mesh.shape["tp"]
    n_x = 2 ** ((n_sp.bit_length() - 1) // 2)
    both, whole = P("sp", "tp"), P()
    return jax.shard_map(
        functools.partial(body, n_sp, n_tp, n_x),
        mesh=mesh,
        in_specs=(both, whole, both, both) + (whole,) * 10 + (both, both),
        out_specs=both,
        check_vma=False,
    )
```

time: 255 us -> 94.1 us (0.37)
  the two profiles are of different devices: /device:TPU:25 before, /device:TPU:1 now
where the time goes in v1:
time: 94.1 us; the launch traced here: 93.7 us
  Pallas kernels  81 us (86%)
  local copies, waits for them, and re-layouts  7.82 us (8%)
  other arithmetic  4.82 us (5%)
    pallas_call x1, Pallas kernels, body(): pl.pallas_call(functools.partial(kernel, n_sp, n_tp, n_x, states), out_sh...  81 us
    dynamic_slice x4, local copies, waits for them, and re-layouts, mine(): return lax.dynamic_slice_in_dim(a, tp * count, count, 0)  4.3 us

profile of v1, /device:TPU:1, one launch (start us, length us, event | category | flops | bytes accessed | tf_op | source)
XLA Modules:
  0.0 93.7 jit_solution(3602262997513431869)
XLA Ops:
  0.0 0.0 copy-start
  0.0 0.0 copy-start.1
  0.0 0.8 exponential_multiply_fusion
  0.8 1.3 %dynamic_slice.37 = f32[256]{0:T(256)} dynamic-slice(f32[1024]{0:T(1024)} %param.27, s32[]{:T(128)S(6)} %select_n.7), dynamic_slice_sizes={256} | dynamic-slice | bytes 2052 | tf_op jit(solution)/shard_map/dynamic_slice | solution.py:387
  2.1 1.3 %dynamic_slice.39 = f32[256]{0:T(256)} dynamic-slice(f32[1024]{0:T(1024)} %param.29, s32[]{:T(128)S(6)} %select_n.7), dynamic_slice_sizes={256} | dynamic-slice | bytes 2052 | tf_op jit(solution)/shard_map/dynamic_slice | solution.py:387
  3.5 0.0 copy-done.1
  3.5 0.8 fusion
  4.3 0.1 stack.28
  4.4 0.8 subtract_divide_fusion
  5.2 0.1 stack.27
  5.3 0.6 pad_maximum_fusion.2.dec_ref
  5.9 0.0 copy-done
  5.9 0.6 constant_dynamic-slice_fusion
  6.6 1.0 %multiply_subtract_fusion = (f32[16,64,16]{1,2,0:T(8,128)S(1)}, f32[16,64,16]{1,2,0:T(8,128)S(1)}) fusion(f32[64,64,16]{1,2,0:T(8,128)} %param.24, s32[]{:T(128)S(6)} %select_n.6, f32[64,64,16]{1,2,0:T(8,128)} %param.23, f32[16,64]{1,0:T(8,128)S(1)} %get-tuple-element.9, f32[16,64]{1,0:T(8,128)S(1)} %get-tuple-element.5), kind=kLoop, calls=%fused_computation.3 | loop fusion | flops 98304 | bytes 270340 | tf_op jit(solution)/shard_map/sub | solution.py:395
  7.6 0.1 stack.30
  7.8 0.1 stack.31
  7.9 1.0 %constant_dynamic-slice_fusion.1 = (f32[16,16,64]{2,1,0:T(8,128)S(1)}, f32[16,16,64]{2,1,0:T(8,128)S(1)}) fusion(f32[64,16,64]{2,1,0:T(8,128)} %param.26, s32[]{:T(128)S(6)} %select_n.6, f32[64,16,64]{2,1,0:T(8,128)} %param.25), kind=kLoop, calls=%fused_computation.15 | loop fusion | bytes 262148 | tf_op jit(solution)/shard_map/dynamic_slice | solution.py:387
  8.9 0.7 pad_maximum_fusion.read_ref
  9.6 1.3 %copy.21.drive_ref = f32[2,1024,16]{2,1,0:T(8,128)} copy(f32[2,1024,16]{1,2,0:T(8,128)S(1)} %pad_maximum_fusion.1) | data formatting | bytes 262144 | tf_op jit(solution)/shard_map/stack | solution.py:393
  10.9 81.0 %shard_map.154 = bf16[256,768]{1,0:T(8,128)(2,1)} custom-call(bf16[256,768]{1,0:T(8,128)(2,1)} %tok_ref.1, f32[1,3072]{1,0:T(1,128)} %bitcast.13, bf16[384,256]{1,0:T(8,128)(2,1)} %wsi_ref.1, bf16[384,256]{1,0:T(8,128)(2,1)} %wpi_ref.1, f32[2,1024]{1,0:T(2,128)} %pad_maximum_fusion.2.dec_ref, f32[2,1024,16]{2,1,0:T(8,128)} %copy.21.drive_ref, ...), custom_call_target="tpu_custom_call" | custom-call | tf_op jit(solution)/shard_map/pallas_call | solution.py:404
  91.9 1.8 %copy.23 = bf16[256,768]{1,0:T(8,128)(2,1)} copy(bf16[256,768]{1,0:T(8,128)(2,1)} %shard_map.154) | data formatting | bytes 786432
  (3 shorter events, 0.1 us)
Async XLA Ops:
  0.0 5.9 %copy-start = (bf16[16,64,64]{2,1,0:T(8,128)(2,1)S(1)}, bf16[16,64,64]{2,1,0:T(8,128)(2,1)}, u32[]{:S(2)}) copy-start(bf16[16,64,64]{2,1,0:T(8,128)(2,1)} %param.28) | copy-start | bytes 393220
  0.0 3.5 %copy-start.1 = (f32[64,64]{1,0:T(8,128)S(1)}, f32[64,64]{1,0:T(8,128)}, u32[]{:S(2)}) copy-start(f32[64,64]{1,0:T(8,128)} %param.21) | copy-start | bytes 49156

commit v2 on v1

--- a/solution.py
+++ b/solution.py
@@ -55,11 +55,11 @@
 
 def kernel(
     n_sp, n_tp, n_x, states,
-    tok_ref, gain_ref, wsi_ref, wpi_ref, dec_ref, drive_ref, read_ref, skip_ref, pw_ref, pg_ref,
-    wso_ref, wpo_ref,
+    tok_ref, gain_ref, wsi_ref, wpi_ref, rr_ref, ri_ref, step_ref, inr_ref, ini_ref, outr_ref,
+    outi_ref, skip_ref, pw_ref, pg_ref, wso_ref, wpo_ref,
     out_ref,
     tok_full, wsi, wpi, wso, wpo, scaled, dmat, rmat, pmat, push, ext, halo, ends, act,
-    mine_s, mine_p, halo_out,
+    mine_s, mine_p, halo_out, rates, matrices, pool_own, dec_ref,
     own_sem, ring_send, ring_recv, tok_send, tok_recv, act_send, act_recv, halo_sem, end_send, end_recv,
 ):
     me, tp = lax.axis_index("sp"), lax.axis_index("tp")
@@ -68,7 +68,9 @@
     features = tok_ref.shape[1]
     width = wsi_ref.shape[1]
     pool_width = wpi_ref.shape[1]
-    columns = dec_ref.shape[1]
+    groups = width // SSM_GROUP
+    columns = groups * states
+    pool_groups = pool_width // POOL_GROUP
     span = rows // CHUNKS
 
     def place(p):
@@ -94,7 +96,20 @@
             )
         )
     owns.append(pltpu.make_async_copy(tok_ref, tok_full.at[tp], own_sem.at[4]))
-    for c in owns:
+    def heads(ref, count):
+        return ref.at[pl.ds(pl.multiple_of(tp * count, count), count)]
+
+    loads = [
+        pltpu.make_async_copy(heads(ref, groups), there, own_sem.at[5 + k])
+        for k, (ref, there) in enumerate(
+            (
+                (rr_ref, rates.at[0]), (ri_ref, rates.at[1]), (inr_ref, matrices.at[0]),
+                (ini_ref, matrices.at[1]), (outr_ref, matrices.at[2]), (outi_ref, matrices.at[3]),
+            )
+        )
+    ]
+    loads.append(pltpu.make_async_copy(heads(pw_ref, pool_groups), pool_own, own_sem.at[11]))
+    for c in owns + loads:
         c.start()
     pl.semaphore_wait(barrier, n_sp - 1 + n_tp - 1)
 
@@ -124,14 +139,21 @@
 
     last = n_sp - 2
 
-    def ring(phase, s):
-        for h in range(PIECES):
-            for a in (2 * phase, 2 * phase + 1):
-                arrive(a, s, h)
-                if s < last:
-                    sender(a, s + 1, h).start()
-                    if s + 1 == last and phase == 0:
-                        sender(a + 2, 0, h).start()
+    def ring(phase, s, h):
+        for a in (2 * phase, 2 * phase + 1):
+            arrive(a, s, h)
+            if s < last:
+                sender(a, s + 1, h).start()
+                if s + 1 == last and phase == 0:
+                    sender(a + 2, 0, h).start()
+
+    turns = [(phase, s, h) for phase in range(2) for s in range(n_sp - 1) for h in range(PIECES)]
+    turn = [0]
+
+    def step(stop=len(turns)):
+        if turn[0] < stop:
+            ring(*turns[turn[0]])
+            turn[0] += 1
 
     def token_copy(k):
         return pltpu.make_async_remote_copy(
@@ -145,29 +167,70 @@
     for k in range(1, n_tp):
         token_copy(k).start()
 
+    tile = iota((states, columns), 0) == iota((states, columns), 1) % states
+    tile_exact, tile_half = tile.astype(f32), tile.astype(bf16)
+
+    def exactly(a, b):
+        return jnp.dot(a, b, precision=lax.Precision.HIGHEST, preferred_element_type=f32)
+
+    factors = []
+
+    def build_decay():
+        for c in loads:
+            c.wait()
+        own_head = iota((groups, columns), 0) == iota((groups, columns), 1) // states
+
+        def flat(a):
+            return jnp.sum(jnp.where(own_head, exactly(a, tile_exact), 0.0), axis=0, keepdims=True)
+
+        rate_real, rate_imag = flat(rates[0]), flat(rates[1])
+        all_groups = step_ref.shape[1]
+        head = iota((all_groups, columns), 0) == tp * groups + iota((all_groups, columns), 1) // states
+        log_step = exactly(jnp.broadcast_to(step_ref[...], (8, all_groups)), head.astype(f32))[0:1]
+        step_size = jnp.exp(log_step) / (rows * n_sp)
+        exponent, angle = rate_real * step_size, rate_imag * step_size
+        magnitude = jnp.exp(exponent)
+        cosine = jnp.cos(angle)
+        decay_real, decay_imag = magnitude * cosine, magnitude * jnp.sin(angle)
+        series = jnp.ones_like(exponent)
+        for k in range(10, 1, -1):
+            series = 1.0 + series * exponent * (1.0 / k)
+        growth = jnp.where(jnp.abs(exponent) < 0.5, exponent * series, magnitude - 1.0)
+        less_one = growth * cosine - 2.0 * jnp.square(jnp.sin(0.5 * angle))
+        denominator = rate_real * rate_real + rate_imag * rate_imag
+        factors.append((less_one * rate_real + decay_imag * rate_imag) / denominator)
+        factors.append((decay_imag * rate_real - less_one * rate_imag) / denominator)
+        dec_ref[0:1, :] = decay_real
+        dec_ref[1:2, :] = decay_imag
+
+    def spread(k):
+        high, low = split(matrices[k].reshape(width, states))
+        return dot(high, tile_half) + dot(low, tile_half)
+
     def build_drive(i):
-        spread = (iota((width, SSM_GROUP), 0) % SSM_GROUP == iota((width, SSM_GROUP), 1)).astype(bf16)
         same = iota((width, columns), 0) // SSM_GROUP == iota((width, columns), 1) // states
-        for j, piece in enumerate(split(drive_ref[i])):
-            dmat[i, j] = jnp.where(same, dot_nt(spread, piece), 0.0).astype(bf16)
+        real, imag = spread(0), spread(1)
+        if i == 0:
+            drive = factors[0] * real - factors[1] * imag
+        else:
+            drive = factors[0] * imag + factors[1] * real
+        for j, piece in enumerate(split(jnp.where(same, drive, 0.0))):
+            dmat[i, j] = piece
 
     def build_read(i):
-        spread = (iota((columns, states), 0) % states == iota((columns, states), 1)).astype(bf16)
+        across = (iota((columns, states), 0) % states == iota((columns, states), 1)).astype(bf16)
         same = iota((columns, width), 0) // states == iota((columns, width), 1) // SSM_GROUP
-        for j, piece in enumerate(split(read_ref[i])):
-            rmat[i, j] = jnp.where(same, dot_nt(spread, piece), 0.0).astype(bf16)
+        for j, piece in enumerate(split(matrices[2 + i].reshape(width, states))):
+            rmat[i, j] = jnp.where(same, dot_nt(across, piece), 0.0).astype(bf16)
 
     def build_pool():
-        spread = (
+        across = (
             iota((POOL_GROUP, pool_width), 0) == iota((POOL_GROUP, pool_width), 1) % POOL_GROUP
         ).astype(bf16)
         same = iota((pool_width, pool_width), 0) // POOL_GROUP == iota((pool_width, pool_width), 1) // POOL_GROUP
-        pmat[...] = jnp.where(same, dot(pw_ref[...], spread), 0.0).astype(bf16)
-
-    first = [
-        lambda: build_drive(0), lambda: build_drive(1), lambda: build_read(0),
-        lambda: build_read(1), build_pool,
-    ]
+        own = pool_own[...].reshape(pool_width, POOL_GROUP)
+        pmat[...] = jnp.where(same, dot(own, across), 0.0).astype(bf16)
+
     squares = []
 
     def take(t):
@@ -184,34 +247,33 @@
                 device_id=(me, (tp + k) % n_tp), device_id_type=MESH,
             ).wait_recv()
 
-    for s in range(n_sp - 1):
-        if s < len(first):
-            first[s]()
-        ring(0, s)
-    for rest in first[n_sp - 1 :]:
-        rest()
+    half = len(turns) // 2
+    for work in (
+        build_decay, lambda: build_drive(0), lambda: build_drive(1), lambda: build_read(0),
+        lambda: build_read(1), build_pool,
+    ):
+        work()
+        step(half)
+    while turn[0] < half - n_tp:
+        step(half)
     tokens_in()
     for t in range(n_tp):
         take(t)
+        step(half)
+    while turn[0] < half:
+        step(half)
     owns[0].wait()
     owns[1].wait()
     inverse = lax.rsqrt(sum(squares) / (features * n_tp) + epsilon)
+    state_in = (dot(scaled[...], wsi[...]) * inverse).astype(bf16)
+    step()
     pool_in = (dot(scaled[...], wpi[...]) * inverse).astype(bf16)
     ext[window_reach:] = pool_in
     halo_out[...] = pool_in[rows - window_reach :]
-    state_in = (dot(scaled[...], wsi[...]) * inverse).astype(bf16)
     halo_copy = pltpu.make_async_remote_copy(
         halo_out, halo, halo_sem.at[0], halo_sem.at[1],
         device_id=((me + 1) % n_sp, tp), device_id_type=MESH,
     )
-    halo_copy.start()
-    done = [0]
-
-    def step():
-        if done[0] < n_sp - 1:
-            ring(1, done[0])
-            done[0] += 1
-
     step()
     shuffle = (
         iota((rows, rows), 1)
@@ -220,7 +282,9 @@
     signal = dot(shuffle, state_in).astype(bf16)
     for i in range(2):
         push[i] = dot(signal, dmat[i, 0]) + dot(signal, dmat[i, 1])
-    step()
+        if i == 0:
+            halo_copy.start()
+        step()
     decay_real = jnp.broadcast_to(dec_ref[0:1, :], (CHUNKS, columns))
     decay_imag = jnp.broadcast_to(dec_ref[1:2, :], (CHUNKS, columns))
 
@@ -276,12 +340,15 @@
         reach = 2**power_index
         band = ((sources <= targets) & (sources > targets - reach)).astype(bf16)
         sums = jnp.where(window == reach, dot(band, whole), sums)
+        if power_index == 2:
+            step()
     position = me * rows + iota((rows, pool_width), 0)
     divisor = jnp.minimum(position + 1, window).astype(f32)
     pooled = sums / divisor - ext[window_reach:].astype(f32)
     pooled_high, pooled_low = split(pooled)
+    pool_gain = pg_ref[:, pl.ds(pl.multiple_of(tp * pool_width, pool_width), pool_width)]
     projected = dot(pooled_high, pmat[...]) + dot(pooled_low, pmat[...])
-    mine_p[...] = (projected * pg_ref[...]).astype(bf16)
+    mine_p[...] = (projected * pool_gain).astype(bf16)
     step()
 
     def act_copy(which, k, source):
@@ -295,6 +362,7 @@
         act_copy(1, k, tp).start()
     act[1, tp] = mine_p[...]
 
+    step()
     for k in range(1, n_sp):
         there = ends.at[(me - k + n_sp) % n_sp]
         pltpu.make_async_remote_copy(
@@ -325,11 +393,14 @@
 
     lax.fori_loop(0, span, add_carry, (begin_real, begin_imag))
     step()
+    step()
     real_high, real_low = split(push[0])
     imag_high, imag_low = split(push[1])
     readout = dot(real_high, rmat[0, 0]) + dot(real_high, rmat[0, 1]) + dot(real_low, rmat[0, 0])
+    step()
     readout -= dot(imag_high, rmat[1, 0]) + dot(imag_high, rmat[1, 1]) + dot(imag_low, rmat[1, 0])
-    readout += skip_ref[...] * signal.astype(f32)
+    skip = skip_ref[:, pl.ds(pl.multiple_of(tp * width, width), width)]
+    readout += skip * signal.astype(f32)
     shuffled = jax.nn.gelu(readout).astype(bf16)
     restore = (
         iota((rows, rows), 0)
@@ -340,7 +411,7 @@
     for k in range(1, n_tp):
         act_copy(0, k, tp).start()
     act[0, tp] = mine_s[...]
-    while done[0] < n_sp - 1:
+    while turn[0] < len(turns):
         step()
     for which in (1, 0):
         for k in range(1, n_tp):
@@ -381,30 +452,14 @@
     states = rate_real.shape[1]
     columns = groups * states
     pool_groups = pool_width // POOL_GROUP
-    tp = lax.axis_index("tp")
-
-    def mine(a, count):
-        return lax.dynamic_slice_in_dim(a, tp * count, count, 0)
-
-    decay_real, decay_imag, factor_real, factor_imag = discretize(
-        mine(rate_real, groups), mine(rate_imag, groups), mine(log_step, groups), rows * n_sp
-    )
-    local_real, local_imag = mine(input_real, groups), mine(input_imag, groups)
-    drive = jnp.stack(
-        [
-            factor_real[..., None] * local_real - factor_imag[..., None] * local_imag,
-            factor_real[..., None] * local_imag + factor_imag[..., None] * local_real,
-        ]
-    ).reshape(2, columns, SSM_GROUP)
-    read = jnp.stack([mine(output_real, groups), mine(output_imag, groups)]).reshape(2, width, states)
-    decay = jnp.stack([decay_real, decay_imag]).reshape(2, columns)
-    pool_matrix = mine(pool_weight, pool_groups).reshape(pool_width, POOL_GROUP)
     vmem = pl.BlockSpec(memory_space=pltpu.VMEM)
+    anywhere = pl.BlockSpec(memory_space=pl.ANY)
     dma = pltpu.SemaphoreType.DMA
     return pl.pallas_call(
         functools.partial(kernel, n_sp, n_tp, n_x, states),
         out_shape=jax.ShapeDtypeStruct((rows, out_columns), bf16),
-        in_specs=[vmem] * 12,
+        in_specs=[anywhere, vmem] + [anywhere] * 4 + [vmem] + [anywhere] * 4 + [vmem, anywhere, vmem]
+        + [anywhere] * 2,
         out_specs=vmem,
         scratch_shapes=[
             pltpu.VMEM((n_tp, rows, features), bf16),
@@ -424,7 +479,11 @@
             pltpu.VMEM((rows, width), bf16),
             pltpu.VMEM((rows, pool_width), bf16),
             pltpu.VMEM((window_reach, pool_width), bf16),
-            dma((5,)),
+            pltpu.VMEM((2, groups, states), f32),
+            pltpu.VMEM((4, groups, SSM_GROUP, states), f32),
+            pltpu.VMEM((pool_groups, POOL_GROUP, POOL_GROUP), bf16),
+            pltpu.VMEM((2, columns), f32),
+            dma((12,)),
             dma((4, n_sp - 1, PIECES)),
             dma((4, n_sp - 1, PIECES)),
             dma((n_tp - 1,)),
@@ -439,9 +498,9 @@
             collective_id=0, has_side_effects=True, vmem_limit_bytes=60 * 2**20
         ),
     )(
-        tokens, norm_gain[None], state_in_weight, pool_in_weight, decay, drive, read,
-        mine(skip_gain, width)[None], pool_matrix, mine(pool_gain, pool_width)[None],
-        state_out_weight, pool_out_weight,
+        tokens, norm_gain[None], state_in_weight, pool_in_weight, rate_real, rate_imag, log_step[None],
+        jnp.swapaxes(input_real, 1, 2), jnp.swapaxes(input_imag, 1, 2), output_real, output_imag,
+        skip_gain[None], pool_weight, pool_gain[None], state_out_weight, pool_out_weight,
     )
 
 

time: 94.1 us -> 82.3 us (0.87)
  local copies, waits for them, and re-layouts: 7.82 us -> 1.77 us
  other arithmetic: 4.82 us -> 0 us
    dynamic_slice x4 -> x0, local copies, waits for them, and re-layouts: 4.3 us -> none  [mine(): return lax.dynamic_slice_in_dim(a, tp * count, count, 0)]
    div x3 -> x0, other arithmetic: 2.48 us -> none  [the longest x1 0.85 us: discretize(): factor_imag = (decay_imag * rate_real - less_one * rate_imag) / denominator]
    another operation x5 -> x0, local copies, waits for them, and re-layouts: 1.66 us -> none  [the longest x3 1.51 us: body(): jnp.stack([factor_real[..., None] * local_real - factor_imag[..., None] *...]
    another operation x3 -> x0, other arithmetic: 1.34 us -> none  [the longest x1 0.72 us: body(): jnp.stack([mine(output_real, groups), mine(output_imag, groups)])]
    sub x1 -> x0, other arithmetic: 1 us -> none  [body(): factor_real[..., None] * local_real - factor_imag[..., None] * local_imag]
where the time goes in v2:
time: 82.3 us; the launch traced here: 82.1 us
  Pallas kernels  80.3 us (98%)
  local copies, waits for them, and re-layouts  1.77 us (2%)
    pallas_call x1, Pallas kernels, body(): pl.pallas_call(functools.partial(kernel, n_sp, n_tp, n_x, states), out_sh...  80.3 us
    unnamed x1, local copies, waits for them, and re-layouts  1.77 us

profile of v2, /device:TPU:1, one launch (start us, length us, event | category | flops | bytes accessed | tf_op | source)
XLA Modules:
  0.0 82.1 jit_solution(4866942636963429740)
XLA Ops:
  0.0 80.3 %shard_map.154 = bf16[256,768]{1,0:T(8,128)(2,1)} custom-call(bf16[256,768]{1,0:T(8,128)(2,1)} %tok_ref.1, f32[1,3072]{1,0:T(1,128)} %bitcast.8, bf16[384,256]{1,0:T(8,128)(2,1)} %wsi_ref.1, bf16[384,256]{1,0:T(8,128)(2,1)} %wpi_ref.1, f32[64,64]{1,0:T(8,128)} %rr_ref.1, f32[64,64]{1,0:T(8,128)} %ri_ref.1, f32[1,64]{1,0:T(1,128)} %bitcast.11, ...), custom_call_target="tpu_custom_call" | custom-call | tf_op jit(solution)/shard_map/pallas_call | solution.py:458
  80.3 1.8 %copy.18 = bf16[256,768]{1,0:T(8,128)(2,1)} copy(bf16[256,768]{1,0:T(8,128)(2,1)} %shard_map.154) | data formatting | bytes 786432

commit v3 on v2

--- a/solution.py
+++ b/solution.py
@@ -113,41 +113,52 @@
         c.start()
     pl.semaphore_wait(barrier, n_sp - 1 + n_tp - 1)
 
-    def part(a, s, h):
+    ways = (1, -1)
+
+    def reach_of(a, d):
+        return n_sp // 2 if a % 2 == d else n_sp - 1 - n_sp // 2
+
+    def part(a, d, s, h):
         own, full = fulls[a]
         count = own.shape[0]
         size = count // PIECES
-        way = 1 if a % 2 == 0 else -1
+        way = ways[d]
         owner = place((at - way * s + n_sp) % n_sp)
         there = full.at[pl.ds(pl.multiple_of(owner * count + h * size, size), size)]
         source = own.at[pl.ds(h * size, size)] if s == 0 else there
         return source, there, (place((at + way + n_sp) % n_sp), tp)
 
-    def sender(a, s, h):
-        source, there, target = part(a, s, h)
+    def sender(a, d, s, h):
+        source, there, target = part(a, d, s, h)
         return pltpu.make_async_remote_copy(
-            source, there, ring_send.at[a, s, h], ring_recv.at[a, s, h],
+            source, there, ring_send.at[a, d, s, h], ring_recv.at[a, d, s, h],
             device_id=target, device_id_type=MESH,
         )
 
-    def arrive(a, s, h):
-        _, there, target = part(a, s + 1, h)
+    def arrive(a, d, s, h):
+        _, there, target = part(a, d, s + 1, h)
         pltpu.make_async_remote_copy(
-            there, there, ring_send.at[a, s, h], ring_recv.at[a, s, h],
+            there, there, ring_send.at[a, d, s, h], ring_recv.at[a, d, s, h],
             device_id=target, device_id_type=MESH,
         ).wait_recv()
 
-    last = n_sp - 2
+    longest = n_sp // 2
 
     def ring(phase, s, h):
-        for a in (2 * phase, 2 * phase + 1):
-            arrive(a, s, h)
-            if s < last:
-                sender(a, s + 1, h).start()
-                if s + 1 == last and phase == 0:
-                    sender(a + 2, 0, h).start()
-
-    turns = [(phase, s, h) for phase in range(2) for s in range(n_sp - 1) for h in range(PIECES)]
+        streams = [
+            (a, d) for a in (2 * phase, 2 * phase + 1) for d in range(2) if s < reach_of(a, d)
+        ]
+        for a, d in sorted(streams, key=lambda i: -reach_of(*i)):
+            arrive(a, d, s, h)
+            if s + 1 < reach_of(a, d):
+                sender(a, d, s + 1, h).start()
+        if phase == 0 and h == PIECES - 1:
+            for a, d in streams:
+                if s + 1 == reach_of(a, d):
+                    for g in range(PIECES):
+                        sender(a + 2, d, 0, g).start()
+
+    turns = [(phase, s, h) for phase in range(2) for s in range(longest) for h in range(PIECES)]
     turn = [0]
 
     def step(stop=len(turns)):
@@ -162,8 +173,8 @@
         )
 
     for h in range(PIECES):
-        for a in (0, 1):
-            sender(a, 0, h).start()
+        for a, d in ((0, 0), (1, 1), (0, 1), (1, 0)):
+            sender(a, d, 0, h).start()
     for k in range(1, n_tp):
         token_copy(k).start()
 
@@ -248,25 +259,28 @@
             ).wait_recv()
 
     half = len(turns) // 2
-    for work in (
-        build_decay, lambda: build_drive(0), lambda: build_drive(1), lambda: build_read(0),
-        lambda: build_read(1), build_pool,
+    for at_work, work in enumerate(
+        (
+            build_decay, lambda: build_drive(0), lambda: build_drive(1), lambda: build_read(0),
+            lambda: build_read(1), build_pool,
+        )
     ):
         work()
-        step(half)
-    while turn[0] < half - n_tp:
+        if at_work in (0, 1, 3, 5):
+            step(half)
+    while turn[0] < half - 3:
         step(half)
     tokens_in()
     for t in range(n_tp):
         take(t)
-        step(half)
+        if t == n_tp // 2 - 1:
+            step(half)
     while turn[0] < half:
         step(half)
     owns[0].wait()
     owns[1].wait()
     inverse = lax.rsqrt(sum(squares) / (features * n_tp) + epsilon)
     state_in = (dot(scaled[...], wsi[...]) * inverse).astype(bf16)
-    step()
     pool_in = (dot(scaled[...], wpi[...]) * inverse).astype(bf16)
     ext[window_reach:] = pool_in
     halo_out[...] = pool_in[rows - window_reach :]
@@ -274,7 +288,6 @@
         halo_out, halo, halo_sem.at[0], halo_sem.at[1],
         device_id=((me + 1) % n_sp, tp), device_id_type=MESH,
     )
-    step()
     shuffle = (
         iota((rows, rows), 1)
         == (iota((rows, rows), 0) % CHUNKS) * span + iota((rows, rows), 0) // CHUNKS
@@ -284,7 +297,8 @@
         push[i] = dot(signal, dmat[i, 0]) + dot(signal, dmat[i, 1])
         if i == 0:
             halo_copy.start()
-        step()
+        else:
+            step()
     decay_real = jnp.broadcast_to(dec_ref[0:1, :], (CHUNKS, columns))
     decay_imag = jnp.broadcast_to(dec_ref[1:2, :], (CHUNKS, columns))
 
@@ -317,7 +331,6 @@
         total = (moved[0] + end_real[j : j + 1], moved[1] + end_imag[j : j + 1])
     which = iota((CHUNKS, columns), 0)
     ends[me] = jnp.where(which == 0, total[0], jnp.where(which == 1, total[1], 0.0))
-    step()
 
     def end_copy(k):
         return pltpu.make_async_remote_copy(
@@ -362,7 +375,6 @@
         act_copy(1, k, tp).start()
     act[1, tp] = mine_p[...]
 
-    step()
     for k in range(1, n_sp):
         there = ends.at[(me - k + n_sp) % n_sp]
         pltpu.make_async_remote_copy(
@@ -392,7 +404,6 @@
         return real, imag
 
     lax.fori_loop(0, span, add_carry, (begin_real, begin_imag))
-    step()
     step()
     real_high, real_low = split(push[0])
     imag_high, imag_low = split(push[1])
@@ -407,7 +418,6 @@
         == (iota((rows, rows), 1) % CHUNKS) * span + iota((rows, rows), 1) // CHUNKS
     ).astype(bf16)
     mine_s[...] = dot(restore, shuffled).astype(bf16)
-    step()
     for k in range(1, n_tp):
         act_copy(0, k, tp).start()
     act[0, tp] = mine_s[...]
@@ -426,9 +436,10 @@
     out_ref[...] = result.astype(bf16)
 
     for a in range(4):
-        for s in range(n_sp - 1):
-            for h in range(PIECES):
-                sender(a, s, h).wait_send()
+        for d in range(2):
+            for s in range(reach_of(a, d)):
+                for h in range(PIECES):
+                    sender(a, d, s, h).wait_send()
     for k in range(1, n_tp):
         token_copy(k).wait_send()
         act_copy(0, k, tp).wait_send()
@@ -484,8 +495,8 @@
             pltpu.VMEM((pool_groups, POOL_GROUP, POOL_GROUP), bf16),
             pltpu.VMEM((2, columns), f32),
             dma((12,)),
-            dma((4, n_sp - 1, PIECES)),
-            dma((4, n_sp - 1, PIECES)),
+            dma((4, 2, n_sp // 2, PIECES)),
+            dma((4, 2, n_sp // 2, PIECES)),
             dma((n_tp - 1,)),
             dma((n_tp - 1,)),
             dma((2, n_tp - 1)),

time: 82.3 us -> 77 us (0.936)
  Pallas kernels: 80.3 us -> 74.8 us
    pallas_call x1, Pallas kernels: 80.3 us -> 74.8 us  [body(): pl.pallas_call(functools.partial(kernel, n_sp, n_tp, n_x, states), out_sh...]
where the time goes in v3:
time: 77 us; the launch traced here: 76.6 us
  Pallas kernels  74.8 us (97%)
  local copies, waits for them, and re-layouts  1.77 us (2%)
    pallas_call x1, Pallas kernels, body(): pl.pallas_call(functools.partial(kernel, n_sp, n_tp, n_x, states), out_sh...  74.8 us
    unnamed x1, local copies, waits for them, and re-layouts  1.77 us

profile of v3, /device:TPU:1, one launch (start us, length us, event | category | flops | bytes accessed | tf_op | source)
XLA Modules:
  0.0 76.6 jit_solution(1755389296602537847)
XLA Ops:
  0.0 74.8 %shard_map.154 = bf16[256,768]{1,0:T(8,128)(2,1)} custom-call(bf16[256,768]{1,0:T(8,128)(2,1)} %tok_ref.1, f32[1,3072]{1,0:T(1,128)} %bitcast.8, bf16[384,256]{1,0:T(8,128)(2,1)} %wsi_ref.1, bf16[384,256]{1,0:T(8,128)(2,1)} %wpi_ref.1, f32[64,64]{1,0:T(8,128)} %rr_ref.1, f32[64,64]{1,0:T(8,128)} %ri_ref.1, f32[1,64]{1,0:T(1,128)} %bitcast.11, ...), custom_call_target="tpu_custom_call" | custom-call | tf_op jit(solution)/shard_map/pallas_call | solution.py:469
  74.8 1.8 %copy.18 = bf16[256,768]{1,0:T(8,128)(2,1)} copy(bf16[256,768]{1,0:T(8,128)(2,1)} %shard_map.154) | data formatting | bytes 786432
